TPU v7x, 512 devices: a whole 4x8x8 slice. The times are simulated.
512 devices in a mesh: sp: 32 (over z, x), tp: 16 (over y, core).
Axes of the slice: x: 4, y: 8, z: 8, core: 2. Of those that a mesh axis runs over, the one named last changes fastest.
Arguments:
- outer_gate: bfloat16 [8192, 2048], P('sp', 'tp'), may hold values from -6 to 6
- inner_gate: bfloat16 [8192, 2048], P('sp', 'tp'), may hold values from -6 to 6
- conv_input: bfloat16 [8192, 2048], P('sp', 'tp'), may hold values from -6 to 6
- conv_weight: bfloat16 [3, 2048], P(None, 'tp'), may hold values from -3.5 to 3.5
- doc_ids: int32 [8192], P('sp'), may hold values from 0 to 15, as said below
- output_weight: bfloat16 [2048, 4096], P(None, 'tp'), may hold values from -0.125 to 0.125
- residual: bfloat16 [8192, 4096], P('sp', 'tp'), as said below
- norm_gain: bfloat16 [4096], P('tp'), may hold values from 0.099609375 to 1.8984375
- expert_ids: int32 [8192, 2], P('sp'), may hold values from 0 to 31, all different within a row; in each aligned block of 256 rows (0 to 255, 256 to 511, ...) at most 32 rows name the same one
- group_weight: float32 [8192], P('sp'), may hold values from 0.25 to 1
- expert_weight: float32 [8192, 2], P('sp'), may hold values from 0.05 to 1
- gate_weight: bfloat16 [32, 4096, 2048], P('sp', None, 'tp'), may hold values from -0.09375 to 0.09375
- up_weight: bfloat16 [32, 4096, 2048], P('sp', None, 'tp'), may hold values from -0.09375 to 0.09375
- down_weight: bfloat16 [32, 2048, 4096], P('sp', None, 'tp'), may hold values from -0.125 to 0.125
Outputs:
- layer_out: bfloat16 [8192, 4096], P('sp', 'tp')
Inputs may be any that keep to these rules, and one draw needn't show every extreme that they name: `expert_ids`: within the 256 rows of one index of sp no expert is named more than 32 times, a bound that some block reaches; the two experts of a row differ. `doc_ids`: never falling along positions, rising by one at each document's start; every document has 256 to 768 positions, and one exactly 768. `residual`: Columns' scales are of order one to ten.
All inputs are finite; a program needn't handle non-finite values.
Results may differ from a plain program's by a relative error of at most 0.009.
Values may be sent and summed in bfloat16 or wider, within the bound.
A program may use at most 64 MiB of HBM per device.

v0:
```python
import jax
import jax.numpy as jnp
from jax import lax
from jax.sharding import PartitionSpec as P

EPS = 1e-06


def passed_along(value, axis, steps):
    count = lax.axis_size(axis)
    initial, last = (max(0, -steps), min(count, count - steps))
    return lax.ppermute(value, axis, [(source, source + steps) for source in range(initial, last)])


def from_everyone(x, axis):
    copies = jnp.broadcast_to(x, (lax.axis_size(axis), *x.shape))
    return lax.all_to_all(copies, axis, split_axis=0, concat_axis=0, tiled=True)


def joined_along(blocks, dim):
    dims = list(blocks.shape[1:])
    dims[dim] *= blocks.shape[0]
    return jnp.moveaxis(blocks, 0, dim).reshape(dims)


def collect(x, axis, dim):
    blocks = from_everyone(x, axis)
    return joined_along(blocks, dim)


def of_everyone(x, axis):
    everything = from_everyone(x, axis)
    return jnp.sum(everything, axis=0)


def per_device(
    outer_gate,
    inner_gate,
    conv_input,
    conv_weight,
    doc_ids,
    output_weight,
    residual,
    norm_gain,
    expert_ids,
    group_weight,
    expert_weight,
    gate_weight,
    up_weight,
    down_weight,
):
    row_count = conv_input.shape[0]
    products = inner_gate.astype(jnp.float32) * conv_input.astype(jnp.float32)
    own_docs = doc_ids.astype(jnp.float32)
    tail_rows, tail_docs = passed_along((products[-2:], own_docs[-2:]), "sp", 1)
    ext_products = jnp.concatenate([tail_rows, products], axis=0)
    ext_docs = jnp.concatenate([tail_docs, own_docs], axis=0)
    taps = conv_weight.astype(jnp.float32)
    conv = taps[2] * products
    for shift_by in (1, 2):
        first = 2 - shift_by
        same_doc = (ext_docs[first : first + row_count] == own_docs)[:, None]
        conv = conv + jnp.where(
            same_doc, taps[2 - shift_by] * ext_products[first : first + row_count], 0.0
        )
    branch = (outer_gate.astype(jnp.float32) * conv).astype(jnp.bfloat16)
    cols_local = output_weight.shape[1]
    branch_sum = jnp.dot(
        collect(branch, "tp", 1), output_weight, preferred_element_type=jnp.float32
    )
    resid = (residual.astype(jnp.float32) + branch_sum).astype(jnp.bfloat16)
    resid_wide = resid.astype(jnp.float32)
    total_sq = of_everyone(jnp.sum(resid_wide * resid_wide, axis=1), "tp")
    width = cols_local * lax.axis_size("tp")
    scale = lax.rsqrt(total_sq / width + EPS)[:, None]
    normed = (resid_wide * scale * norm_gain.astype(jnp.float32)).astype(jnp.bfloat16)
    experts = lax.axis_size("sp")
    capacity = 4 * row_count // experts
    flat_experts = expert_ids.reshape(-1)
    onehot = (flat_experts[:, None] == jnp.arange(experts, dtype=jnp.int32)[None, :]).astype(
        jnp.int32
    )
    slot_rank = jnp.sum((jnp.cumsum(onehot, axis=0) - onehot) * onehot, axis=1)
    slot_index = flat_experts * capacity + slot_rank
    token_of = jnp.arange(2 * row_count, dtype=jnp.int32) // 2
    token_table = jnp.full((experts * capacity,), row_count, jnp.int32).at[slot_index].set(token_of)
    gate_local = gate_weight[0]
    up_local = up_weight[0]
    arrived_rows = experts * capacity
    padded = jnp.concatenate([normed, jnp.zeros((1, cols_local), jnp.bfloat16)], axis=0)
    outgoing = padded[token_table].reshape(experts, capacity, cols_local)
    arrived = lax.all_to_all(outgoing, "sp", split_axis=0, concat_axis=0, tiled=True).reshape(
        arrived_rows, cols_local
    )
    piece = lax.all_gather(arrived, "tp", axis=1, tiled=True)
    gate_val = jnp.dot(piece, gate_local, preferred_element_type=jnp.float32)
    up_val = jnp.dot(piece, up_local, preferred_element_type=jnp.float32)
    hidden = (jax.nn.silu(gate_val) * up_val).astype(jnp.bfloat16)
    down_local = down_weight[0]
    expert_out = jnp.dot(
        lax.all_gather(hidden, "tp", axis=1, tiled=True),
        down_local,
        preferred_element_type=jnp.float32,
    ).astype(jnp.bfloat16)
    returned = lax.all_to_all(
        expert_out.reshape(experts, capacity, cols_local),
        "sp",
        split_axis=0,
        concat_axis=0,
        tiled=True,
    )
    picked = (
        returned.reshape(arrived_rows, cols_local)[slot_index]
        .reshape(row_count, 2, cols_local)
        .astype(jnp.float32)
    )
    mix_weight = (
        group_weight[:, None] * expert_weight / jnp.sum(expert_weight, axis=1, keepdims=True)
    )
    routed_sum = jnp.sum(picked * mix_weight[:, :, None], axis=1)
    return (resid_wide + routed_sum).astype(jnp.bfloat16)


def solution(mesh):
    return jax.shard_map(
        per_device,
        mesh=mesh,
        in_specs=(
            P("sp", "tp"),
            P("sp", "tp"),
            P("sp", "tp"),
            P(None, "tp"),
            P("sp"),
            P(None, "tp"),
            P("sp", "tp"),
            P("tp"),
            P("sp", None),
            P("sp"),
            P("sp", None),
            P("sp", None, "tp"),
            P("sp", None, "tp"),
            P("sp", None, "tp"),
        ),
        out_specs=P("sp", "tp"),
        check_vma=False,
    )
```

profile of v0, /device:TPU:8, one launch (start us, length us, event | category | flops | bytes accessed | tf_op | source)
XLA Modules:
  0.0 263.7 jit_solution(17630297964401948509)
XLA Ops:
  6.5 0.8 convert_element_type.60
  7.4 3.4 %collective-permute-start = (f32[2]{0:T(128)S(1)}, f32[2]{0:T(128)S(1)}, u32[]{:S(2)}, u32[]{:S(2)}) collective-permute-start(f32[2]{0:T(128)S(1)} %slice.34), channel_id=1, source_target_pairs={{0,16},{16,32},{32,48},{48,64},{64,80},{80,96},{96,112},{112,128},... | collective-permute-start | bytes 32 | tf_op jit(solution)/shard_map/ppermute | solution.py:12
  10.8 0.9 convert_multiply_fusion
  11.7 3.4 %collective-permute-start.1 = (f32[2,128]{1,0:T(2,128)S(1)}, f32[2,128]{1,0:T(2,128)S(1)}, u32[]{:S(2)}, u32[]{:S(2)}) collective-permute-start(f32[2,128]{1,0:T(2,128)S(1)} %slice.48), channel_id=1, source_target_pairs={{0,16},{16,32},{32,48},{48,64},{64,80},{80,96},{96,112},{112,128},... | collective-permute-start | bytes 3080 | tf_op jit(solution)/shard_map/ppermute | solution.py:12
  16.7 1.0 fusion.13
  17.8 1.1 broadcast_in_dim.44
  18.9 7.6 %all-to-all-start = ((bf16[16,256,128]{1,2,0:T(8,128)(2,1)}), bf16[16,256,128]{1,2,0:T(8,128)(2,1)S(1)}, u32[]{:S(2)}, u32[]{:S(2)}) async-start(bf16[16,256,128]{1,2,0:T(8,128)(2,1)} %broadcast_in_dim.44), calls=%async_computation | async-start | bytes 2097152 | tf_op jit(solution)/shard_map/all_to_all | solution.py:17
  26.4 0.8 copy.31
  27.5 1.2 reduce-window.6
  30.1 2.4 scatter_custom_fusion
  32.5 18.5 %all-to-all-done = bf16[16,256,128]{1,2,0:T(8,128)(2,1)S(1)} async-done(((bf16[16,256,128]{1,2,0:T(8,128)(2,1)}), bf16[16,256,128]{1,2,0:T(8,128)(2,1)S(1)}, u32[]{:S(2)}, u32[]{:S(2)}) %all-to-all-start) | async-done | bytes 1048608 | tf_op jit(solution)/shard_map/all_to_all | solution.py:17
  51.0 1.8 multiply_reduce_fusion.1
  53.5 6.8 %all-to-all-start.1 = ((f32[16,1,256]{2,1,0:T(1,128)}), f32[16,1,256]{2,1,0:T(1,128)S(1)}, u32[]{:S(2)}, u32[]{:S(2)}) async-start(f32[16,1,256]{2,1,0:T(1,128)} %broadcast_in_dim.45), calls=%async_computation.1 | async-start | bytes 32768 | tf_op jit(solution)/shard_map/all_to_all | solution.py:17
  61.0 5.5 %all-to-all-done.1 = f32[16,1,256]{2,1,0:T(1,128)S(1)} async-done(((f32[16,1,256]{2,1,0:T(1,128)}), f32[16,1,256]{2,1,0:T(1,128)S(1)}, u32[]{:S(2)}, u32[]{:S(2)}) %all-to-all-start.1) | async-done | bytes 16416 | tf_op jit(solution)/shard_map/all_to_all | solution.py:17
  66.7 3.9 %gather_fusion = bf16[1024,256]{1,0:T(8,128)(2,1)S(1)} fusion(bf16[257,256]{1,0:T(8,128)(2,1)S(1)} %concatenate.11, s32[1024]{0:T(1024)S(1)} %fusion.20), kind=kCustom, calls=%fused_computation | custom fusion | bytes 1052672 | tf_op jit(solution)/shard_map/gather | solution.py:91
  70.7 32.5 %all_to_all.21 = bf16[32,32,256]{2,1,0:T(8,128)(2,1)} all-to-all(bf16[32,32,256]{2,1,0:T(8,128)(2,1)S(1)} %bitcast.51), channel_id=1, replica_groups=mesh['sp'=32,'tp'=16] {'sp'}, dimensions={0} | all-to-all | bytes 1048576 | tf_op jit(solution)/shard_map/all_to_all | solution.py:92
  103.2 58.8 %all-gather.3.cloned.1.call-done = bf16[1024,4096]{1,0:T(8,128)(2,1)} async-done(((bf16[1024,256]{1,0:T(8,128)(2,1)}), bf16[1024,4096]{1,0:T(8,128)(2,1)}) %all-gather.3.cloned.1.call-update) | async-done | bytes 8388624 | tf_op jit(solution)/shard_map/all_gather | solution.py:95
  162.0 5.9 %fusion.5 = f32[1024,128]{1,0:T(8,128)S(1)} fusion(bf16[1024,4096]{1,0:T(8,128)(2,1)} %all-gather.3.cloned.1.call-done, bf16[1,4096,128]{2,1,0:T(8,128)(2,1)S(1)} %copy-done.4), kind=kOutput, calls=%fused_computation.11 | convolution fusion | flops 1073741824 | bytes 9961472 | tf_op jit(solution)/shard_map/dot_general | solution.py:96
  168.0 3.0 %fusion = bf16[1024,128]{1,0:T(8,128)(2,1)} fusion(bf16[1024,4096]{1,0:T(8,128)(2,1)S(1)} %copy-done.3, bf16[1,4096,128]{2,1,0:T(8,128)(2,1)S(1)} %copy-done.5, f32[1024,128]{1,0:T(8,128)S(1)} %fusion.5), kind=kOutput, calls=%fused_computation.5 | convolution fusion | flops 1074528256 | bytes 10223616 | tf_op jit(solution)/shard_map/dot_general | solution.py:97
  171.0 49.6 %all-gather.5.cloned.1.call-done = bf16[1024,2048]{1,0:T(8,128)(2,1)} async-done(((bf16[1024,128]{1,0:T(8,128)(2,1)}), bf16[1024,2048]{1,0:T(8,128)(2,1)}) %all-gather.5.cloned.1.call-update) | async-done | bytes 4194320 | tf_op jit(solution)/shard_map/all_gather | solution.py:101
  220.6 4.2 %convolution_convert_fusion = bf16[1024,256]{1,0:T(8,128)(2,1)} fusion(bf16[1024,2048]{1,0:T(8,128)(2,1)} %all-gather.5.cloned.1.call-done, bf16[1,2048,256]{2,1,0:T(8,128)(2,1)S(1)} %copy-done), kind=kOutput, calls=%fused_computation.3 | convolution fusion | flops 1074003968 | bytes 5767168 | tf_op jit(solution)/shard_map/dot_general | solution.py:100
  224.9 10.2 %all-to-all-start.3 = ((bf16[32,32,256]{2,1,0:T(8,128)(2,1)}), bf16[32,32,256]{2,1,0:T(8,128)(2,1)S(1)}, u32[]{:S(2)}, u32[]{:S(2)}) async-start(bf16[32,32,256]{2,1,0:T(8,128)(2,1)} %bitcast.13), calls=%async_computation.3 | async-start | bytes 1048576 | tf_op jit(solution)/shard_map/all_to_all | solution.py:105
  235.3 18.0 %all-to-all-done.3 = bf16[32,32,256]{2,1,0:T(8,128)(2,1)S(1)} async-done(((bf16[32,32,256]{2,1,0:T(8,128)(2,1)}), bf16[32,32,256]{2,1,0:T(8,128)(2,1)S(1)}, u32[]{:S(2)}, u32[]{:S(2)}) %all-to-all-start.3) | async-done | bytes 524320 | tf_op jit(solution)/shard_map/all_to_all | solution.py:105
  253.3 1.9 gather_fusion.1
  (51 shorter events, 6.9 us)
Async XLA Ops:
  6.5 214.1 %copy-start = (bf16[1,2048,256]{2,1,0:T(8,128)(2,1)S(1)}, bf16[1,2048,256]{2,1,0:T(8,128)(2,1)}, u32[]{:S(2)}) copy-start(bf16[1,2048,256]{2,1,0:T(8,128)(2,1)} %param.27) | copy-start | bytes 3145732
  6.5 155.5 %copy-start.4 = (bf16[1,4096,128]{2,1,0:T(8,128)(2,1)S(1)}, bf16[1,4096,128]{2,1,0:T(8,128)(2,1)}, u32[]{:S(2)}) copy-start(bf16[1,4096,128]{2,1,0:T(8,128)(2,1)} %param.25) | copy-start | bytes 3145732
  7.4 8.4 %collective-permute-start = (f32[2]{0:T(128)S(1)}, f32[2]{0:T(128)S(1)}, u32[]{:S(2)}, u32[]{:S(2)}) collective-permute-start(f32[2]{0:T(128)S(1)} %slice.34), channel_id=1, source_target_pairs={{0,16},{16,32},{32,48},{48,64},{64,80},{80,96},{96,112},{112,128},... | collective-permute-start | bytes 32 | tf_op jit(solution)/shard_map/ppermute | solution.py:12
  11.7 4.9 %collective-permute-start.1 = (f32[2,128]{1,0:T(2,128)S(1)}, f32[2,128]{1,0:T(2,128)S(1)}, u32[]{:S(2)}, u32[]{:S(2)}) collective-permute-start(f32[2,128]{1,0:T(2,128)S(1)} %slice.48), channel_id=1, source_target_pairs={{0,16},{16,32},{32,48},{48,64},{64,80},{80,96},{96,112},{112,128},... | collective-permute-start | bytes 3080 | tf_op jit(solution)/shard_map/ppermute | solution.py:12
  18.9 32.2 %all-to-all-start = ((bf16[16,256,128]{1,2,0:T(8,128)(2,1)}), bf16[16,256,128]{1,2,0:T(8,128)(2,1)S(1)}, u32[]{:S(2)}, u32[]{:S(2)}) async-start(bf16[16,256,128]{1,2,0:T(8,128)(2,1)} %broadcast_in_dim.44), calls=%async_computation | async-start | bytes 2097152 | tf_op jit(solution)/shard_map/all_to_all | solution.py:17
  53.5 13.1 %all-to-all-start.1 = ((f32[16,1,256]{2,1,0:T(1,128)}), f32[16,1,256]{2,1,0:T(1,128)S(1)}, u32[]{:S(2)}, u32[]{:S(2)}) async-start(f32[16,1,256]{2,1,0:T(1,128)} %broadcast_in_dim.45), calls=%async_computation.1 | async-start | bytes 32768 | tf_op jit(solution)/shard_map/all_to_all | solution.py:17
  60.3 101.7 %all-gather.3.cloned.1.call-start = ((), (), s32[]{:S(2)}) async-start(), calls=%async_computation.4 | async-start | bytes 8912896 | tf_op jit(solution)/shard_map/all_gather | solution.py:95
  103.2 117.4 %all-gather.5.cloned.1.call-start = ((), (), s32[]{:S(2)}) async-start(), calls=%async_computation.5 | async-start | bytes 4456448 | tf_op jit(solution)/shard_map/all_gather | solution.py:101
  162.0 5.9 %copy-start.3 = (bf16[1024,4096]{1,0:T(8,128)(2,1)S(1)}, bf16[1024,4096]{1,0:T(8,128)(2,1)}, u32[]{:S(2)}) copy-start(bf16[1024,4096]{1,0:T(8,128)(2,1)} %all-gather.3.cloned.1.call-done) | copy-start | bytes 25165828
  162.0 6.0 %copy-start.5 = (bf16[1,4096,128]{2,1,0:T(8,128)(2,1)S(1)}, bf16[1,4096,128]{2,1,0:T(8,128)(2,1)}, u32[]{:S(2)}) copy-start(bf16[1,4096,128]{2,1,0:T(8,128)(2,1)} %param.26) | copy-start | bytes 3145732
  168.0 67.1 %copy-start.1 = (f32[256,2]{0,1:T(2,128)S(1)}, f32[256,2]{0,1:T(2,128)}, u32[]{:S(2)}) copy-start(f32[256,2]{0,1:T(2,128)} %param.24) | copy-start | bytes 6148
  168.0 67.1 %copy-start.2 = (f32[256]{0:T(256)S(1)}, f32[256]{0:T(256)}, u32[]{:S(2)}) copy-start(f32[256]{0:T(256)} %param.23) | copy-start | bytes 3076
  224.9 28.4 %all-to-all-start.3 = ((bf16[32,32,256]{2,1,0:T(8,128)(2,1)}), bf16[32,32,256]{2,1,0:T(8,128)(2,1)S(1)}, u32[]{:S(2)}, u32[]{:S(2)}) async-start(bf16[32,32,256]{2,1,0:T(8,128)(2,1)} %bitcast.13), calls=%async_computation.3 | async-start | bytes 1048576 | tf_op jit(solution)/shard_map/all_to_all | solution.py:105
Sparse Core Ops, SparseCore 0:
  103.3 58.6 all-gather.2
  171.2 49.4 all-gather.4
where the time goes:
time: 264 us
  waiting for transfers between devices  150 us (57%)
  blocking collectives  32.5 us (12%)
  starting transfers between devices  31.4 us (12%)
  matrix products  14.9 us (6%)
  between operations  13.6 us (5%)
  local copies, waits for them, and re-layouts  12.4 us (5%)
  other arithmetic  8.46 us (3%)
    all_gather x1, waiting for transfers between devices, per_device(): piece = lax.all_gather(arrived, 'tp', axis=1, tiled=True)  58.8 us
    all_gather x1, waiting for transfers between devices, per_device(): lax.all_gather(hidden, 'tp', axis=1, tiled=True)  49.6 us
    all_to_all x1, blocking collectives, per_device(): lax.all_to_all(outgoing, 'sp', split_axis=0, concat_axis=0, tiled=True)  32.5 us
    all_to_all x2, waiting for transfers between devices, from_everyone(): return lax.all_to_all(copies, axis, split_axis=0, concat_axis=0, tiled=True)  24 us
    all_to_all x1, waiting for transfers between devices, per_device(): lax.all_to_all(expert_out.reshape(experts, capacity, cols_local), 'sp', s...  18 us
    all_to_all x2, starting transfers between devices, from_everyone(): return lax.all_to_all(copies, axis, split_axis=0, concat_axis=0, tiled=True)  14.4 us
    all_to_all x1, starting transfers between devices, per_device(): lax.all_to_all(expert_out.reshape(experts, capacity, cols_local), 'sp', s...  10.2 us
    ppermute x2, starting transfers between devices, passed_along(): lax.ppermute(value, axis, [(source, source + steps) for source in range(i...  6.78 us
  transfers between devices with their start and end apart: 7, of which 5 were waited for; matrix products, arithmetic and copies ran while one was open for 4% of the time, Pallas kernels for 0%

commit v1 on v0

--- a/solution.py
+++ b/solution.py
@@ -1,9 +1,46 @@
+import functools
 import jax
 import jax.numpy as jnp
 from jax import lax
 from jax.sharding import PartitionSpec as P
 
 EPS = 1e-06
+
+
+def leaves_remake(xs, d0, peer_axis):
+    arr_out, tall, heard = (
+        jax.lax.axis_size(peer_axis),
+        jax.lax.axis_index(peer_axis),
+        xs.shape[d0],
+    )
+    sides = []
+    nth = 0
+    while nth < arr_out:
+        sides.append((nth, (nth + 1) % arr_out))
+        nth = nth + 1
+    fields = []
+    nth = 0
+    while nth < arr_out:
+        fields.append((nth, (nth - 1) % arr_out))
+        nth = nth + 1
+    then = jnp.zeros((*xs.shape[:d0], arr_out * heard, *xs.shape[d0 + 1 :]), xs.dtype)
+    then = lax.dynamic_update_slice_in_dim(then, xs, tall * heard, axis=d0)
+    main = v_next = xs
+    carry_out = arr_out // 2
+    q = 1
+    while q < carry_out + 1:
+        main = jax.lax.ppermute(main, peer_axis, sides)
+        then = lax.dynamic_update_slice_in_dim(then, main, (tall - q) % arr_out * heard, axis=d0)
+        if q < arr_out - carry_out:
+            v_next = jax.lax.ppermute(v_next, peer_axis, fields)
+            then = lax.dynamic_update_slice_in_dim(
+                then, v_next, (tall + q) % arr_out * heard, axis=d0
+            )
+        q += 1
+    return then
+
+
+manage_circles = functools.partial(leaves_remake, d0=1, peer_axis="tp")
 
 
 def passed_along(value, axis, steps):
@@ -92,7 +129,7 @@
     arrived = lax.all_to_all(outgoing, "sp", split_axis=0, concat_axis=0, tiled=True).reshape(
         arrived_rows, cols_local
     )
-    piece = lax.all_gather(arrived, "tp", axis=1, tiled=True)
+    piece = manage_circles(arrived)
     gate_val = jnp.dot(piece, gate_local, preferred_element_type=jnp.float32)
     up_val = jnp.dot(piece, up_local, preferred_element_type=jnp.float32)
     hidden = (jax.nn.silu(gate_val) * up_val).astype(jnp.bfloat16)

time: 264 us -> 275 us (1.042)
  starting transfers between devices: 31.4 us -> 45.4 us
  local copies, waits for them, and re-layouts: 12.4 us -> 17.5 us
  waiting for transfers between devices: 150 us -> 145 us
  matrix products: 14.9 us -> 11.4 us
    all_gather x1 -> x0, waiting for transfers between devices: 58.8 us -> none  [per_device(): piece = lax.all_gather(arrived, 'tp', axis=1, tiled=True)]
    ppermute x0 -> x15, waiting for transfers between devices: none -> 52.1 us  [the longest x8 49 us: leaves_remake(): main = jax.lax.ppermute(main, peer_axis, sides)]
    ppermute x0 -> x15, starting transfers between devices: none -> 14.1 us  [the longest x7 14.1 us: leaves_remake(): v_next = jax.lax.ppermute(v_next, peer_axis, fields)]
    dynamic_update_slice x0 -> x16, local copies, waits for them, and re-layouts: none -> 4.16 us  [the longest x8 2.6 us: leaves_remake(): lax.dynamic_update_slice_in_dim(then, main, (tall - q) % arr_out * heard,...]
    dot_general x1, matrix products: 5.86 us -> 2.34 us  [per_device(): gate_val = jnp.dot(piece, gate_local, preferred_element_type=jnp.float32)]
  transfers between devices with their start and end apart: 7 -> 21, of which waited for: 5 -> 16; matrix products, arithmetic and copies ran while one was open for 4% -> 5% of each run, Pallas kernels for 0% -> 0%
where the time goes in v1:
time: 275 us; the launch traced here: 274 us
  waiting for transfers between devices  145 us (53%)
  starting transfers between devices  45.4 us (17%)
  blocking collectives  32.4 us (12%)
  local copies, waits for them, and re-layouts  17.5 us (6%)
  between operations  13.9 us (5%)
  matrix products  11.4 us (4%)
  other arithmetic  8.4 us (3%)
    all_gather x1, waiting for transfers between devices, per_device(): lax.all_gather(hidden, 'tp', axis=1, tiled=True)  50.7 us
    ppermute x8, waiting for transfers between devices, leaves_remake(): main = jax.lax.ppermute(main, peer_axis, sides)  49 us
    all_to_all x1, blocking collectives, per_device(): lax.all_to_all(outgoing, 'sp', split_axis=0, concat_axis=0, tiled=True)  32.4 us
    all_to_all x2, waiting for transfers between devices, from_everyone(): return lax.all_to_all(copies, axis, split_axis=0, concat_axis=0, tiled=True)  24 us
    all_to_all x1, waiting for transfers between devices, per_device(): lax.all_to_all(expert_out.reshape(experts, capacity, cols_local), 'sp', s...  18 us
    all_to_all x2, starting transfers between devices, from_everyone(): return lax.all_to_all(copies, axis, split_axis=0, concat_axis=0, tiled=True)  14.4 us
    ppermute x7, starting transfers between devices, leaves_remake(): v_next = jax.lax.ppermute(v_next, peer_axis, fields)  14.1 us
    all_to_all x1, starting transfers between devices, per_device(): lax.all_to_all(expert_out.reshape(experts, capacity, cols_local), 'sp', s...  10.2 us
  transfers between devices with their start and end apart: 21, of which 16 were waited for; matrix products, arithmetic and copies ran while one was open for 5% of the time, Pallas kernels for 0%

profile of v1, /device:TPU:8, one launch (start us, length us, event | category | flops | bytes accessed | tf_op | source)
XLA Modules:
  0.0 273.8 jit_solution(10590167379694517775)
XLA Ops:
  7.4 3.4 %collective-permute-start = (f32[2]{0:T(128)S(1)}, f32[2]{0:T(128)S(1)}, u32[]{:S(2)}, u32[]{:S(2)}) collective-permute-start(f32[2]{0:T(128)S(1)} %slice.34), channel_id=1, source_target_pairs={{0,16},{16,32},{32,48},{48,64},{64,80},{80,96},{96,112},{112,128},... | collective-permute-start | bytes 32 | tf_op jit(solution)/shard_map/ppermute | solution.py:49
  11.7 3.4 %collective-permute-start.1 = (f32[2,128]{1,0:T(2,128)S(1)}, f32[2,128]{1,0:T(2,128)S(1)}, u32[]{:S(2)}, u32[]{:S(2)}) collective-permute-start(f32[2,128]{1,0:T(2,128)S(1)} %slice.48), channel_id=1, source_target_pairs={{0,16},{16,32},{32,48},{48,64},{64,80},{80,96},{96,112},{112,128},... | collective-permute-start | bytes 3080 | tf_op jit(solution)/shard_map/ppermute | solution.py:49
  18.8 7.6 %all-to-all-start = ((bf16[16,256,128]{1,2,0:T(8,128)(2,1)}), bf16[16,256,128]{1,2,0:T(8,128)(2,1)S(1)}, u32[]{:S(2)}, u32[]{:S(2)}) async-start(bf16[16,256,128]{1,2,0:T(8,128)(2,1)} %broadcast_in_dim.47), calls=%async_computation | async-start | bytes 2097152 | tf_op jit(solution)/shard_map/all_to_all | solution.py:54
  30.0 2.4 scatter_custom_fusion
  32.5 18.5 %all-to-all-done = bf16[16,256,128]{1,2,0:T(8,128)(2,1)S(1)} async-done(((bf16[16,256,128]{1,2,0:T(8,128)(2,1)}), bf16[16,256,128]{1,2,0:T(8,128)(2,1)S(1)}, u32[]{:S(2)}, u32[]{:S(2)}) %all-to-all-start) | async-done | bytes 1048608 | tf_op jit(solution)/shard_map/all_to_all | solution.py:54
  53.4 6.8 %all-to-all-start.1 = ((f32[16,1,256]{2,1,0:T(1,128)}), f32[16,1,256]{2,1,0:T(1,128)S(1)}, u32[]{:S(2)}, u32[]{:S(2)}) async-start(f32[16,1,256]{2,1,0:T(1,128)} %broadcast_in_dim.49), calls=%async_computation.1 | async-start | bytes 32768 | tf_op jit(solution)/shard_map/all_to_all | solution.py:54
  60.9 5.5 %all-to-all-done.1 = f32[16,1,256]{2,1,0:T(1,128)S(1)} async-done(((f32[16,1,256]{2,1,0:T(1,128)}), f32[16,1,256]{2,1,0:T(1,128)S(1)}, u32[]{:S(2)}, u32[]{:S(2)}) %all-to-all-start.1) | async-done | bytes 16416 | tf_op jit(solution)/shard_map/all_to_all | solution.py:54
  66.6 3.9 %gather_fusion = bf16[1024,256]{1,0:T(8,128)(2,1)S(1)} fusion(bf16[257,256]{1,0:T(8,128)(2,1)S(1)} %concatenate.11, s32[1024]{0:T(1024)S(1)} %fusion.20), kind=kCustom, calls=%fused_computation | custom fusion | bytes 1052672 | tf_op jit(solution)/shard_map/gather | solution.py:128
  70.6 32.4 %all_to_all.21 = bf16[32,32,256]{2,1,0:T(8,128)(2,1)S(1)} all-to-all(bf16[32,32,256]{2,1,0:T(8,128)(2,1)S(1)} %bitcast.55), channel_id=1, replica_groups=mesh['sp'=32,'tp'=16] {'sp'}, dimensions={0} | all-to-all | bytes 1048576 | tf_op jit(solution)/shard_map/all_to_all | solution.py:129
  104.7 6.9 %collective-permute-done.2 = bf16[1024,256]{1,0:T(8,128)(2,1)S(1)} collective-permute-done((bf16[1024,256]{1,0:T(8,128)(2,1)S(1)}, bf16[1024,256]{1,0:T(8,128)(2,1)S(1)}, u32[]{:S(2)}, u32[]{:S(2)}) %collective-permute-start.2) | collective-permute-done | bytes 524320 | tf_op jit(solution)/shard_map/ppermute | solution.py:32
  113.6 6.6 %collective-permute-done.4 = bf16[1024,256]{1,0:T(8,128)(2,1)S(1)} collective-permute-done((bf16[1024,256]{1,0:T(8,128)(2,1)S(1)}, bf16[1024,256]{1,0:T(8,128)(2,1)S(1)}, u32[]{:S(2)}, u32[]{:S(2)}) %collective-permute-start.4) | collective-permute-done | bytes 524320 | tf_op jit(solution)/shard_map/ppermute | solution.py:32
  122.5 6.3 %collective-permute-done.6 = bf16[1024,256]{1,0:T(8,128)(2,1)S(1)} collective-permute-done((bf16[1024,256]{1,0:T(8,128)(2,1)S(1)}, bf16[1024,256]{1,0:T(8,128)(2,1)S(1)}, u32[]{:S(2)}, u32[]{:S(2)}) %collective-permute-start.6) | collective-permute-done | bytes 524320 | tf_op jit(solution)/shard_map/ppermute | solution.py:32
  131.4 6.1 %collective-permute-done.8 = bf16[1024,256]{1,0:T(8,128)(2,1)} collective-permute-done((bf16[1024,256]{1,0:T(8,128)(2,1)S(1)}, bf16[1024,256]{1,0:T(8,128)(2,1)}, u32[]{:S(2)}, u32[]{:S(2)}) %collective-permute-start.8) | collective-permute-done | bytes 524320 | tf_op jit(solution)/shard_map/ppermute | solution.py:32
  138.1 2.3 collective-permute-start.11
  140.5 6.0 %collective-permute-done.10 = bf16[1024,256]{1,0:T(8,128)(2,1)} collective-permute-done((bf16[1024,256]{1,0:T(8,128)(2,1)}, bf16[1024,256]{1,0:T(8,128)(2,1)}, u32[]{:S(2)}, u32[]{:S(2)}) %collective-permute-start.10) | collective-permute-done | bytes 524320 | tf_op jit(solution)/shard_map/ppermute | solution.py:32
  149.7 5.5 %collective-permute-done.12 = bf16[1024,256]{1,0:T(8,128)(2,1)S(1)} collective-permute-done((bf16[1024,256]{1,0:T(8,128)(2,1)}, bf16[1024,256]{1,0:T(8,128)(2,1)S(1)}, u32[]{:S(2)}, u32[]{:S(2)}) %collective-permute-start.12) | collective-permute-done | bytes 524320 | tf_op jit(solution)/shard_map/ppermute | solution.py:32
  160.5 3.4 %collective-permute-done.14 = bf16[1024,256]{1,0:T(8,128)(2,1)S(1)} collective-permute-done((bf16[1024,256]{1,0:T(8,128)(2,1)S(1)}, bf16[1024,256]{1,0:T(8,128)(2,1)S(1)}, u32[]{:S(2)}, u32[]{:S(2)}) %collective-permute-start.14) | collective-permute-done | bytes 524320 | tf_op jit(solution)/shard_map/ppermute | solution.py:32
  166.2 8.3 %collective-permute-done.16 = bf16[1024,256]{1,0:T(8,128)(2,1)S(1)} collective-permute-done((bf16[1024,256]{1,0:T(8,128)(2,1)S(1)}, bf16[1024,256]{1,0:T(8,128)(2,1)S(1)}, u32[]{:S(2)}, u32[]{:S(2)}) %collective-permute-start.16) | collective-permute-done | bytes 524320 | tf_op jit(solution)/shard_map/ppermute | solution.py:32
  174.6 2.3 fusion.5
  177.0 3.0 %multiply_convert_fusion = bf16[1024,128]{1,0:T(8,128)(2,1)} fusion(f32[1024,128]{1,0:T(8,128)S(1)} %fusion.5, bf16[1024,4096]{1,0:T(8,128)(2,1)S(1)} %constant_dynamic-update-slice_fusion, bf16[1,4096,128]{2,1,0:T(8,128)(2,1)S(1)} %copy-done.12), kind=kOutput, calls=%fused_computation.13 | convolution fusion | flops 1074528256 | bytes 10223616 | tf_op jit(solution)/shard_map/dot_general | solution.py:134
  180.0 50.7 %all-gather.2.cloned.1.call-done = bf16[1024,2048]{1,0:T(8,128)(2,1)} async-done(((bf16[1024,128]{1,0:T(8,128)(2,1)}), bf16[1024,2048]{1,0:T(8,128)(2,1)}) %all-gather.2.cloned.1.call-update) | async-done | bytes 4194320 | tf_op jit(solution)/shard_map/all_gather | solution.py:138
  230.7 4.2 %convolution_convert_fusion = bf16[1024,256]{1,0:T(8,128)(2,1)} fusion(bf16[1024,2048]{1,0:T(8,128)(2,1)} %all-gather.2.cloned.1.call-done, bf16[1,2048,256]{2,1,0:T(8,128)(2,1)S(1)} %copy-done), kind=kOutput, calls=%fused_computation.3 | convolution fusion | flops 1074003968 | bytes 5767168 | tf_op jit(solution)/shard_map/dot_general | solution.py:137
  235.0 10.2 %all-to-all-start.3 = ((bf16[32,32,256]{2,1,0:T(8,128)(2,1)}), bf16[32,32,256]{2,1,0:T(8,128)(2,1)S(1)}, u32[]{:S(2)}, u32[]{:S(2)}) async-start(bf16[32,32,256]{2,1,0:T(8,128)(2,1)} %bitcast.13), calls=%async_computation.3 | async-start | bytes 1048576 | tf_op jit(solution)/shard_map/all_to_all | solution.py:142
  245.4 18.0 %all-to-all-done.3 = bf16[32,32,256]{2,1,0:T(8,128)(2,1)S(1)} async-done(((bf16[32,32,256]{2,1,0:T(8,128)(2,1)}), bf16[32,32,256]{2,1,0:T(8,128)(2,1)S(1)}, u32[]{:S(2)}, u32[]{:S(2)}) %all-to-all-start.3) | async-done | bytes 524320 | tf_op jit(solution)/shard_map/all_to_all | solution.py:142
  (109 shorter events, 36.2 us)
Async XLA Ops:
  6.5 224.2 %copy-start = (bf16[1,2048,256]{2,1,0:T(8,128)(2,1)S(1)}, bf16[1,2048,256]{2,1,0:T(8,128)(2,1)}, u32[]{:S(2)}) copy-start(bf16[1,2048,256]{2,1,0:T(8,128)(2,1)} %param.27) | copy-start | bytes 3145732
  7.4 8.4 %collective-permute-start = (f32[2]{0:T(128)S(1)}, f32[2]{0:T(128)S(1)}, u32[]{:S(2)}, u32[]{:S(2)}) collective-permute-start(f32[2]{0:T(128)S(1)} %slice.34), channel_id=1, source_target_pairs={{0,16},{16,32},{32,48},{48,64},{64,80},{80,96},{96,112},{112,128},... | collective-permute-start | bytes 32 | tf_op jit(solution)/shard_map/ppermute | solution.py:49
  11.7 4.9 %collective-permute-start.1 = (f32[2,128]{1,0:T(2,128)S(1)}, f32[2,128]{1,0:T(2,128)S(1)}, u32[]{:S(2)}, u32[]{:S(2)}) collective-permute-start(f32[2,128]{1,0:T(2,128)S(1)} %slice.48), channel_id=1, source_target_pairs={{0,16},{16,32},{32,48},{48,64},{64,80},{80,96},{96,112},{112,128},... | collective-permute-start | bytes 3080 | tf_op jit(solution)/shard_map/ppermute | solution.py:49
  18.8 32.2 %all-to-all-start = ((bf16[16,256,128]{1,2,0:T(8,128)(2,1)}), bf16[16,256,128]{1,2,0:T(8,128)(2,1)S(1)}, u32[]{:S(2)}, u32[]{:S(2)}) async-start(bf16[16,256,128]{1,2,0:T(8,128)(2,1)} %broadcast_in_dim.47), calls=%async_computation | async-start | bytes 2097152 | tf_op jit(solution)/shard_map/all_to_all | solution.py:54
  53.4 13.1 %all-to-all-start.1 = ((f32[16,1,256]{2,1,0:T(1,128)}), f32[16,1,256]{2,1,0:T(1,128)S(1)}, u32[]{:S(2)}, u32[]{:S(2)}) async-start(f32[16,1,256]{2,1,0:T(1,128)} %broadcast_in_dim.49), calls=%async_computation.1 | async-start | bytes 32768 | tf_op jit(solution)/shard_map/all_to_all | solution.py:54
  60.2 170.5 %all-gather.2.cloned.1.call-start = ((), (), s32[]{:S(2)}) async-start(), calls=%async_computation.4 | async-start | bytes 4456448 | tf_op jit(solution)/shard_map/all_gather | solution.py:138
  103.0 8.6 %collective-permute-start.2 = (bf16[1024,256]{1,0:T(8,128)(2,1)S(1)}, bf16[1024,256]{1,0:T(8,128)(2,1)S(1)}, u32[]{:S(2)}, u32[]{:S(2)}) collective-permute-start(bf16[1024,256]{1,0:T(8,128)(2,1)S(1)} %bitcast.52), channel_id=1, source_target_pairs={{0,1},{1,2},{2,3},{3,4},{4,5},{5,6},{6,7},{7,8},{8,9},{9,10},{10,1... | collective-permute-start | bytes 1572872 | tf_op jit(solution)/shard_map/ppermute | solution.py:32
  103.0 8.6 %collective-permute-start.3 = (bf16[1024,256]{1,0:T(8,128)(2,1)S(1)}, bf16[1024,256]{1,0:T(8,128)(2,1)S(1)}, u32[]{:S(2)}, u32[]{:S(2)}) collective-permute-start(bf16[1024,256]{1,0:T(8,128)(2,1)S(1)} %bitcast.53), channel_id=1, source_target_pairs={{0,15},{1,0},{2,1},{3,2},{4,3},{5,4},{6,5},{7,6},{8,7},{9,8},{10,9... | collective-permute-start | bytes 1572872 | tf_op jit(solution)/shard_map/ppermute | solution.py:35
  111.6 8.6 %collective-permute-start.4 = (bf16[1024,256]{1,0:T(8,128)(2,1)S(1)}, bf16[1024,256]{1,0:T(8,128)(2,1)S(1)}, u32[]{:S(2)}, u32[]{:S(2)}) collective-permute-start(bf16[1024,256]{1,0:T(8,128)(2,1)S(1)} %collective-permute-done.2), channel_id=1, source_target_pairs={{0,1},{1,2},{2,3},{3,4},{4,5},{5,6},{6,7},{7,8},{8,9},{9,10},{10,1... | collective-permute-start | bytes 1572872 | tf_op jit(solution)/shard_map/ppermute | solution.py:32
  111.6 8.7 %collective-permute-start.5 = (bf16[1024,256]{1,0:T(8,128)(2,1)S(1)}, bf16[1024,256]{1,0:T(8,128)(2,1)S(1)}, u32[]{:S(2)}, u32[]{:S(2)}) collective-permute-start(bf16[1024,256]{1,0:T(8,128)(2,1)S(1)} %collective-permute-done.3), channel_id=1, source_target_pairs={{0,15},{1,0},{2,1},{3,2},{4,3},{5,4},{6,5},{7,6},{8,7},{9,8},{10,9... | collective-permute-start | bytes 1572872 | tf_op jit(solution)/shard_map/ppermute | solution.py:35
  120.2 8.6 %collective-permute-start.6 = (bf16[1024,256]{1,0:T(8,128)(2,1)S(1)}, bf16[1024,256]{1,0:T(8,128)(2,1)S(1)}, u32[]{:S(2)}, u32[]{:S(2)}) collective-permute-start(bf16[1024,256]{1,0:T(8,128)(2,1)S(1)} %collective-permute-done.4), channel_id=1, source_target_pairs={{0,1},{1,2},{2,3},{3,4},{4,5},{5,6},{6,7},{7,8},{8,9},{9,10},{10,1... | collective-permute-start | bytes 1572872 | tf_op jit(solution)/shard_map/ppermute | solution.py:32
  120.3 8.9 %collective-permute-start.7 = (bf16[1024,256]{1,0:T(8,128)(2,1)S(1)}, bf16[1024,256]{1,0:T(8,128)(2,1)S(1)}, u32[]{:S(2)}, u32[]{:S(2)}) collective-permute-start(bf16[1024,256]{1,0:T(8,128)(2,1)S(1)} %collective-permute-done.5), channel_id=1, source_target_pairs={{0,15},{1,0},{2,1},{3,2},{4,3},{5,4},{6,5},{7,6},{8,7},{9,8},{10,9... | collective-permute-start | bytes 1572872 | tf_op jit(solution)/shard_map/ppermute | solution.py:35
  128.8 8.7 %collective-permute-start.8 = (bf16[1024,256]{1,0:T(8,128)(2,1)S(1)}, bf16[1024,256]{1,0:T(8,128)(2,1)}, u32[]{:S(2)}, u32[]{:S(2)}) collective-permute-start(bf16[1024,256]{1,0:T(8,128)(2,1)S(1)} %collective-permute-done.6), channel_id=1, source_target_pairs={{0,1},{1,2},{2,3},{3,4},{4,5},{5,6},{6,7},{7,8},{8,9},{9,10},{10,1... | collective-permute-start | bytes 1572872 | tf_op jit(solution)/shard_map/ppermute | solution.py:32
  129.2 8.9 %collective-permute-start.9 = (bf16[1024,256]{1,0:T(8,128)(2,1)S(1)}, bf16[1024,256]{1,0:T(8,128)(2,1)}, u32[]{:S(2)}, u32[]{:S(2)}) collective-permute-start(bf16[1024,256]{1,0:T(8,128)(2,1)S(1)} %collective-permute-done.7), channel_id=1, source_target_pairs={{0,15},{1,0},{2,1},{3,2},{4,3},{5,4},{6,5},{7,6},{8,7},{9,8},{10,9... | collective-permute-start | bytes 1572872 | tf_op jit(solution)/shard_map/ppermute | solution.py:35
  137.5 8.9 %collective-permute-start.10 = (bf16[1024,256]{1,0:T(8,128)(2,1)}, bf16[1024,256]{1,0:T(8,128)(2,1)}, u32[]{:S(2)}, u32[]{:S(2)}) collective-permute-start(bf16[1024,256]{1,0:T(8,128)(2,1)} %collective-permute-done.8), channel_id=1, source_target_pairs={{0,1},{1,2},{2,3},{3,4},{4,5},{5,6},{6,7},{7,8},{8,9},{9,10},{10,1... | collective-permute-start | bytes 1572872 | tf_op jit(solution)/shard_map/ppermute | solution.py:32
  138.1 9.7 %collective-permute-start.11 = (bf16[1024,256]{1,0:T(8,128)(2,1)}, bf16[1024,256]{1,0:T(8,128)(2,1)S(1)}, u32[]{:S(2)}, u32[]{:S(2)}) collective-permute-start(bf16[1024,256]{1,0:T(8,128)(2,1)} %collective-permute-done.9), channel_id=1, source_target_pairs={{0,15},{1,0},{2,1},{3,2},{4,3},{5,4},{6,5},{7,6},{8,7},{9,8},{10,9... | collective-permute-start | bytes 1572872 | tf_op jit(solution)/shard_map/ppermute | solution.py:35
  146.4 8.8 %collective-permute-start.12 = (bf16[1024,256]{1,0:T(8,128)(2,1)}, bf16[1024,256]{1,0:T(8,128)(2,1)S(1)}, u32[]{:S(2)}, u32[]{:S(2)}) collective-permute-start(bf16[1024,256]{1,0:T(8,128)(2,1)} %collective-permute-done.10), channel_id=1, source_target_pairs={{0,1},{1,2},{2,3},{3,4},{4,5},{5,6},{6,7},{7,8},{8,9},{9,10},{10,1... | collective-permute-start | bytes 1572872 | tf_op jit(solution)/shard_map/ppermute | solution.py:32
  147.8 9.8 %collective-permute-start.13 = (bf16[1024,256]{1,0:T(8,128)(2,1)S(1)}, bf16[1024,256]{1,0:T(8,128)(2,1)S(1)}, u32[]{:S(2)}, u32[]{:S(2)}) collective-permute-start(bf16[1024,256]{1,0:T(8,128)(2,1)S(1)} %collective-permute-done.11), channel_id=1, source_target_pairs={{0,15},{1,0},{2,1},{3,2},{4,3},{5,4},{6,5},{7,6},{8,7},{9,8},{10,9... | collective-permute-start | bytes 1572872 | tf_op jit(solution)/shard_map/ppermute | solution.py:35
  155.3 8.6 %collective-permute-start.14 = (bf16[1024,256]{1,0:T(8,128)(2,1)S(1)}, bf16[1024,256]{1,0:T(8,128)(2,1)S(1)}, u32[]{:S(2)}, u32[]{:S(2)}) collective-permute-start(bf16[1024,256]{1,0:T(8,128)(2,1)S(1)} %collective-permute-done.12), channel_id=1, source_target_pairs={{0,1},{1,2},{2,3},{3,4},{4,5},{5,6},{6,7},{7,8},{8,9},{9,10},{10,1... | collective-permute-start | bytes 1572872 | tf_op jit(solution)/shard_map/ppermute | solution.py:32
  157.7 8.5 %collective-permute-start.15 = (bf16[1024,256]{1,0:T(8,128)(2,1)S(1)}, bf16[1024,256]{1,0:T(8,128)(2,1)S(1)}, u32[]{:S(2)}, u32[]{:S(2)}) collective-permute-start(bf16[1024,256]{1,0:T(8,128)(2,1)S(1)} %collective-permute-done.13), channel_id=1, source_target_pairs={{0,15},{1,0},{2,1},{3,2},{4,3},{5,4},{6,5},{7,6},{8,7},{9,8},{10,9... | collective-permute-start | bytes 1572872 | tf_op jit(solution)/shard_map/ppermute | solution.py:35
  163.9 10.6 %collective-permute-start.16 = (bf16[1024,256]{1,0:T(8,128)(2,1)S(1)}, bf16[1024,256]{1,0:T(8,128)(2,1)S(1)}, u32[]{:S(2)}, u32[]{:S(2)}) collective-permute-start(bf16[1024,256]{1,0:T(8,128)(2,1)S(1)} %collective-permute-done.14), channel_id=1, source_target_pairs={{0,1},{1,2},{2,3},{3,4},{4,5},{5,6},{6,7},{7,8},{8,9},{9,10},{10,1... | collective-permute-start | bytes 1572872 | tf_op jit(solution)/shard_map/ppermute | solution.py:32
  177.0 68.2 %copy-start.9 = (f32[256,2]{0,1:T(2,128)S(1)}, f32[256,2]{0,1:T(2,128)}, u32[]{:S(2)}) copy-start(f32[256,2]{0,1:T(2,128)} %param.24) | copy-start | bytes 6148
  177.0 68.2 %copy-start.10 = (f32[256]{0:T(256)S(1)}, f32[256]{0:T(256)}, u32[]{:S(2)}) copy-start(f32[256]{0:T(256)} %param.23) | copy-start | bytes 3076
  235.0 28.4 %all-to-all-start.3 = ((bf16[32,32,256]{2,1,0:T(8,128)(2,1)}), bf16[32,32,256]{2,1,0:T(8,128)(2,1)S(1)}, u32[]{:S(2)}, u32[]{:S(2)}) async-start(bf16[32,32,256]{2,1,0:T(8,128)(2,1)} %bitcast.13), calls=%async_computation.3 | async-start | bytes 1048576 | tf_op jit(solution)/shard_map/all_to_all | solution.py:142
  (10 other events, 137.0 us)
Sparse Core Ops, SparseCore 0:
  180.2 50.5 all-gather.1
